TPU v7x, 512 devices: a whole 4x8x8 slice. The times are simulated.
512 devices in a mesh: kv: 128 (over z, y, core), tp: 4 (over x).
Axes of the slice: x: 4, y: 8, z: 8, core: 2. Of those that a mesh axis runs over, the one named last changes fastest.
Arguments:
- tokens: bfloat16 [65536, 2048], P('kv'), may hold values from -18 to 18
- w_query: bfloat16 [2048, 1024], P(None, 'tp'), may hold values from -0.125 to 0.125
- w_key: bfloat16 [2048, 256], P(None, 'tp'), may hold values from -0.125 to 0.125
- w_value: bfloat16 [2048, 256], P(None, 'tp'), may hold values from -18 to 18
- w_out: bfloat16 [1024, 2048], P(None, 'tp'), may hold values from -0.1875 to 0.1875
- out_gain: float32 [1024], replicated, may hold values from 0.1 to 1.9
- chosen: int32 [4, 1024, 8], P('tp', 'kv'), may hold values from -1 to 1023, as said below
Outputs:
- mixed_out: bfloat16 [65536, 2048], P('kv', 'tp')
Inputs may be any that keep to these rules, and one draw needn't show every extreme that they name: chosen[h, b, 0] is b itself; the other entries of a row are distinct key blocks lying wholly before block b, or -1, placed after all named blocks; for each key head h, the query blocks on one index of kv (its 512 positions) name, together, at most one key block of head h held by any other index of kv.
All inputs are finite; a program needn't handle non-finite values.
Results may differ from a plain program's by a relative error of at most 0.024.
Values may be sent and summed in bfloat16 or wider, within the bound.
A program may use at most 64 MiB of HBM per device.

v0:
```python
import jax
import jax.numpy as jnp
from jax import lax
from jax.sharding import Mesh
from jax.sharding import PartitionSpec as P

HQ = 16
HD = 64
BLK = 64
SEL = 8
KV = ("kv_0", "kv_1", "kv_2")


rope_base = 500000.0
norm_eps = 1e-06


def cut_along(array, dim, count):
    shape = array.shape
    pieces = array.reshape(*shape[:dim], count, shape[dim] // count, *shape[dim + 1 :])
    return jnp.moveaxis(pieces, dim, 0)


def laid_out(pieces, dim):
    pieces = jnp.moveaxis(pieces, 0, dim)
    shape = pieces.shape
    return pieces.reshape(*shape[:dim], shape[dim] * shape[dim + 1], *shape[dim + 2 :])


def turned_blocks(pieces, axes, turns):
    inside = pieces.shape[1:]
    whole = pieces.reshape(*(lax.axis_size(a) for a in axes), *inside)
    for k in turns:
        whole = lax.all_to_all(whole, axes[k], k, k, tiled=True)
    return whole.reshape(-1, *inside)


def two_step_exchange(array, groups, turns, split_dim, concat_dim):
    count = lax.axis_size(groups[0]) * lax.axis_size(groups[1])
    pieces = cut_along(array, split_dim, count)
    return laid_out(turned_blocks(pieces, groups, turns), concat_dim)


def from_everyone(array, axis):
    copies = jnp.broadcast_to(array, (lax.axis_size(axis), *array.shape))
    return lax.all_to_all(copies, axis, split_axis=0, concat_axis=0, tiled=True)


def collect(array, axis, dim):
    return laid_out(from_everyone(array, axis), dim)


def rotate(vectors, positions):
    half_size = vectors.shape[-1] // 2
    frequency = rope_base ** (-jnp.arange(half_size, dtype=jnp.float32) / half_size)
    angles = positions.astype(jnp.float32)[:, None] * frequency[None, :]
    cosine = jnp.cos(angles)[:, None, :]
    sine_wave = jnp.sin(angles)[:, None, :]
    lower_half = vectors[..., :half_size]
    upper_half = vectors[..., half_size:]
    return jnp.concatenate(
        [
            lower_half * cosine - upper_half * sine_wave,
            upper_half * cosine + lower_half * sine_wave,
        ],
        axis=-1,
    )


def per_device(tokens, w_query, w_key, w_value, w_out, out_gain, chosen):
    count_kv = lax.axis_size(KV)
    kv_place = lax.axis_index(KV)
    row_count = tokens.shape[0]
    block_count = row_count // BLK
    feat_width = w_query.shape[1]
    head_count = feat_width // HD
    positions = kv_place * row_count + jnp.arange(row_count, dtype=jnp.int32)
    queries = rotate(
        jnp.dot(tokens, w_query, preferred_element_type=jnp.float32).reshape(
            row_count, head_count, HD
        ),
        positions,
    ).astype(jnp.bfloat16)
    key_rows = (
        rotate(
            jnp.dot(tokens, w_key, preferred_element_type=jnp.float32).reshape(row_count, 1, HD),
            positions,
        )
        .astype(jnp.bfloat16)
        .reshape(row_count, HD)
    )
    value_rows = jnp.dot(tokens, w_value, preferred_element_type=jnp.float32).astype(jnp.bfloat16)
    local_pairs = jnp.concatenate([key_rows, value_rows], axis=1).reshape(block_count, BLK, 2 * HD)
    chosen_ids = chosen[0]
    usable = chosen_ids >= 0
    owners = jnp.where(usable, chosen_ids // block_count, kv_place)
    local_index = jnp.where(usable, chosen_ids % block_count, 0)
    remote = usable & (owners != kv_place)
    peer_ids = jnp.arange(count_kv, dtype=jnp.int32)
    matches = remote[:, :, None] & (owners[:, :, None] == peer_ids[None, None, :])
    wanted = jnp.max(jnp.where(matches, local_index[:, :, None], -1), axis=(0, 1))
    asked_for = two_step_exchange(
        wanted.reshape(count_kv, 1), (("kv_0", "kv_1"), "kv_2"), (1, 0), 0, 0
    )[:, 0]
    outgoing = jnp.where(
        (asked_for >= 0)[:, None, None],
        local_pairs[jnp.maximum(asked_for, 0)],
        jnp.zeros((), jnp.bfloat16),
    )
    arrived = lax.all_to_all(outgoing, KV, split_axis=0, concat_axis=0, tiled=True)
    pool_pairs = jnp.concatenate([arrived, local_pairs], axis=0)
    slot_index = jnp.where(owners == kv_place, count_kv + local_index, owners)
    selected = pool_pairs[slot_index]
    pair_count = block_count // 2
    offsets = jnp.arange(BLK, dtype=jnp.int32)
    score_scale = HD ** (-0.5)

    def attend(bundle):
        query_part, stacked, pair_ids, pair_usable, query_pos = bundle
        key_part = stacked[..., :HD]
        value_part = stacked[..., HD:]
        scores = (
            jnp.einsum("pqhd,pskd->phqsk", query_part, key_part, preferred_element_type=jnp.float32)
            * score_scale
        )
        key_pos = pair_ids[:, :, None] * BLK + offsets
        allowed = pair_usable[:, None, :, None] & (
            key_pos[:, None, :, :] <= query_pos[:, :, None, None]
        )
        scores = jnp.where(allowed[:, None], scores, -jnp.inf)
        peak_score = jnp.max(scores, axis=(3, 4), keepdims=True)
        weights = jnp.exp(scores - peak_score)
        softmax_w = (weights / jnp.sum(weights, axis=(3, 4), keepdims=True)).astype(jnp.bfloat16)
        mixed_out = jnp.einsum(
            "phqsk,pskd->pqhd", softmax_w, value_part, preferred_element_type=jnp.float32
        )
        return mixed_out.astype(jnp.bfloat16)

    attended = lax.map(
        attend,
        (
            queries.reshape(pair_count, 2, BLK, head_count, HD),
            selected.reshape(pair_count, 2, SEL, BLK, 2 * HD),
            chosen_ids.reshape(pair_count, 2, SEL),
            usable.reshape(pair_count, 2, SEL),
            positions.reshape(pair_count, 2, BLK),
        ),
    ).reshape(row_count, feat_width)
    cols_f32 = collect(attended, "tp", 1).astype(jnp.float32)
    scaled = (cols_f32 * out_gain[None, :]).astype(jnp.bfloat16)
    product = jnp.dot(scaled, w_out, preferred_element_type=jnp.float32)
    squares = jnp.sum(cols_f32 * cols_f32, axis=1)
    inverse = lax.rsqrt(squares / (HQ * HD) + norm_eps)
    return (inverse[:, None] * product).astype(jnp.bfloat16)


def solution(mesh):
    finer = Mesh(mesh.devices.reshape(8, 8, 2, mesh.shape["tp"]), ("kv_0", "kv_1", "kv_2", "tp"))
    placed = (
        P(KV, None),
        P(None, "tp"),
        P(None, "tp"),
        P(None, "tp"),
        P(None, "tp"),
        P(),
        P("tp", KV, None),
    )
    return jax.shard_map(
        per_device, mesh=finer, in_specs=placed, out_specs=P(KV, "tp"), check_vma=False
    )
```

profile of v0, /device:TPU:8, one launch (start us, length us, event | category | flops | bytes accessed | tf_op | source)
XLA Modules:
  0.0 147.7 jit_solution(6819352520383450894)
XLA Ops:
  0.0 0.8 fusion.20
  0.9 0.7 compare_and_fusion.1
  1.9 3.7 %all_to_all.20 = s32[64,2,1,1]{0,3,2,1:T(1,128)S(1)} all-to-all(s32[64,2,1,1]{0,3,2,1:T(1,128)S(1)} %copy.31), channel_id=1, replica_groups=mesh['kv_0'=8,'kv_1'=8,'kv_2'=2,'tp'=4] {'kv_2'}, dimensions={1} | all-to-all | bytes 1024 | tf_op jit(solution)/shard_map/all_to_all | solution.py:34
  5.6 0.7 copy.32
  6.3 16.6 %all-to-all-start.1 = ((s32[64,2,1,1]{1,3,2,0:T(1,128)}), s32[64,2,1,1]{1,3,2,0:T(1,128)S(1)}, u32[]{:S(2)}, u32[]{:S(2)}) async-start(s32[64,2,1,1]{1,3,2,0:T(1,128)} %copy.32), calls=%async_computation.1 | async-start | bytes 65536 | tf_op jit(solution)/shard_map/all_to_all | solution.py:34
  22.9 1.7 %convolution_bitcast_fusion.1 = f32[512,1,64]{0,2,1:T(8,128)S(1)} fusion(bf16[512,2048]{1,0:T(8,128)(2,1)S(1)} %copy-done, bf16[2048,64]{0,1:T(8,128)(2,1)} %param.11), kind=kOutput, calls=%fused_computation.31 | convolution fusion | flops 134217728 | bytes 2490368 | tf_op jit(solution)/shard_map/dot_general | solution.py:86
  25.2 0.8 convolution_convert_fusion
  26.3 7.6 %all-to-all-done.1 = s32[64,2,1,1]{1,3,2,0:T(1,128)S(1)} async-done(((s32[64,2,1,1]{1,3,2,0:T(1,128)}), s32[64,2,1,1]{1,3,2,0:T(1,128)S(1)}, u32[]{:S(2)}, u32[]{:S(2)}) %all-to-all-start.1) | async-done | bytes 544 | tf_op jit(solution)/shard_map/all_to_all | solution.py:34
  34.4 2.2 %gather_fusion = bf16[128,64,128]{2,1,0:T(8,128)(2,1)} fusion(bf16[8,64,128]{2,1,0:T(8,128)(2,1)S(1)} %pad_maximum_fusion.1, s32[1024]{0:T(1024)S(1)} %pad_clamp_fusion.1), kind=kCustom, calls=%fused_computation | custom fusion | bytes 4194816 | tf_op jit(solution)/shard_map/gather | solution.py:107
  36.5 3.2 %broadcast_select_fusion = bf16[128,64,128]{2,1,0:T(8,128)(2,1)} fusion(bf16[128,64,128]{2,1,0:T(8,128)(2,1)} %gather_fusion, pred[128]{0:T(512)(128)(4,1)S(1)} %ge.36), kind=kLoop, calls=%fused_computation.28 | loop fusion | flops 1048576 | bytes 4194432 | tf_op jit(solution)/shard_map/jit(_where)/select_n | solution.py:105
  39.7 7.8 %all-to-all-start.2 = ((bf16[128,64,128]{2,1,0:T(8,128)(2,1)}), bf16[128,64,128]{2,1,0:T(8,128)(2,1)}, u32[]{:S(2)}, u32[]{:S(2)}) async-start(bf16[128,64,128]{2,1,0:T(8,128)(2,1)} %broadcast_select_fusion), calls=%async_computation.2 | async-start | bytes 4194304 | tf_op jit(solution)/shard_map/all_to_all | solution.py:110
  48.0 2.0 %fusion.34 = f32[512,256]{0,1:T(8,128)S(1)} fusion(bf16[512,2048]{1,0:T(8,128)(2,1)S(1)} %copy-done, bf16[2048,256]{1,0:T(8,128)(2,1)} %param.10), kind=kOutput, calls=%fused_computation.94 | convolution fusion | flops 536870912 | bytes 3670016 | tf_op jit(solution)/shard_map/dot_general | solution.py:79
  50.4 1.6 %pad_maximum_fusion = bf16[4,2,64,4,64]{2,1,0,4,3:T(2,128)(2,1)} fusion(bf16[4,2,64,4,32]{2,1,0,4,3:T(2,128)(2,1)S(1)} %concatenate.35, bf16[4,2,64,4,32]{2,1,0,4,3:T(2,128)(2,1)S(1)} %concatenate.34), kind=kLoop, calls=%fused_computation.33 | loop fusion | flops 131072 | bytes 524288 | tf_op jit(solution)/shard_map/concatenate | solution.py:61
  52.1 49.2 %all-to-all-done.2 = bf16[128,64,128]{2,1,0:T(8,128)(2,1)} async-done(((bf16[128,64,128]{2,1,0:T(8,128)(2,1)}), bf16[128,64,128]{2,1,0:T(8,128)(2,1)}, u32[]{:S(2)}, u32[]{:S(2)}) %all-to-all-start.2) | async-done | bytes 2097184 | tf_op jit(solution)/shard_map/all_to_all | solution.py:110
  101.3 3.6 %maximum_maximum_fusion = bf16[136,64,128]{2,1,0:T(8,128)(2,1)} fusion(bf16[8,64,64]{2,1,0:T(8,128)(2,1)S(1)} %bitcast.157, bf16[8,64,32]{2,1,0:T(8,128)(2,1)S(1)} %bitcast.155, bf16[8,64,32]{2,1,0:T(8,128)(2,1)S(1)} %bitcast.153, bf16[128,64,128]{2,1,0:T(8,128)(2,1)} %all-to-all-done.2), kind=kLoop, calls=%fused_computation.24 | loop fusion | flops 8912896 | bytes 4456448 | tf_op jit(solution)/shard_map/concatenate | solution.py:111
  104.9 2.4 %gather_fusion.1 = bf16[64,64,128]{2,1,0:T(8,128)(2,1)S(1)} fusion(bf16[136,64,128]{2,1,0:T(8,128)(2,1)} %maximum_maximum_fusion, s32[1024]{0:T(1024)S(1)} %pad_clamp_fusion), kind=kCustom, calls=%fused_computation.1 | custom fusion | bytes 2097408 | tf_op jit(solution)/shard_map/gather | solution.py:113
  107.3 17.6 %while.11 = (s32[]{:T(128)}, bf16[4,2,64,4,64]{2,1,0,4,3:T(2,128)(2,1)}, bf16[4,2,8,64,128]{4,3,2,1,0:T(8,128)(2,1)S(1)}, pred[4,2,8]{2,1,0:T(4,128)(4,1)S(1)}, ...) while((s32[]{:T(128)}, ...), condition=%wide.region_4.5_spmd.clone, body=%wide.region_1.4_spmd.clone.sunk | while | flops 69369872 | bytes 13324689 | solution.py:139
  108.3 1.0 constant_dynamic-slice_fusion.4
  110.9 0.8 copy_dynamic-update-slice_fusion.2
  112.1 0.6 copy-done.1
  112.7 1.0 constant_dynamic-slice_fusion.4
  115.3 0.8 copy_dynamic-update-slice_fusion.2
  116.5 0.6 copy-done.1
  117.1 1.0 constant_dynamic-slice_fusion.4
  119.8 0.8 copy_dynamic-update-slice_fusion.2
  120.9 0.6 copy-done.1
  121.5 1.0 constant_dynamic-slice_fusion.4
  124.1 0.8 copy_dynamic-update-slice_fusion.2
  124.9 1.4 reshape.383
  126.4 18.5 %all_to_all.21 = bf16[4,512,256]{1,2,0:T(8,128)(2,1)S(1)} all-to-all(bf16[4,512,256]{1,2,0:T(8,128)(2,1)S(1)} %broadcast_in_dim.86), channel_id=1, replica_groups=mesh['kv_0'=8,'kv_1'=8,'kv_2'=2,'tp'=4] {'tp'}, dimensions={0} | all-to-all | bytes 2097152 | tf_op jit(solution)/shard_map/all_to_all | solution.py:46
  145.5 0.6 copy-done.6
  146.2 1.5 %fusion.10 = bf16[512,512]{1,0:T(8,128)(2,1)} fusion(bf16[512,1024]{0,1:T(8,128)(2,1)S(1)} %fusion.9, bf16[1024,512]{1,0:T(8,128)(2,1)S(1)} %copy-done.6, f32[512]{0:T(512)S(1)} %add_rsqrt_fusion), kind=kOutput, calls=%fused_computation.30 | convolution fusion | flops 537395200 | bytes 2623488 | tf_op jit(solution)/shard_map/dot_general | solution.py:151
  (91 shorter events, 11.5 us)
Async XLA Ops:
  0.0 22.9 %copy-start = (bf16[512,2048]{1,0:T(8,128)(2,1)S(1)}, bf16[512,2048]{1,0:T(8,128)(2,1)}, u32[]{:S(2)}) copy-start(bf16[512,2048]{1,0:T(8,128)(2,1)} %param.9) | copy-start | bytes 6291460
  0.0 25.2 %copy-start.3 = (bf16[2048,64]{0,1:T(8,128)(2,1)S(1)}, bf16[2048,64]{0,1:T(8,128)(2,1)}, u32[]{:S(2)}) copy-start(bf16[2048,64]{0,1:T(8,128)(2,1)} %param.12) | copy-start | bytes 786436
  6.3 27.6 %all-to-all-start.1 = ((s32[64,2,1,1]{1,3,2,0:T(1,128)}), s32[64,2,1,1]{1,3,2,0:T(1,128)S(1)}, u32[]{:S(2)}, u32[]{:S(2)}) async-start(s32[64,2,1,1]{1,3,2,0:T(1,128)} %copy.32), calls=%async_computation.1 | async-start | bytes 65536 | tf_op jit(solution)/shard_map/all_to_all | solution.py:34
  39.7 7.8 %copy-start.4 = (s32[1,8,8]{2,1,0:T(8,128)S(1)}, s32[1,8,8]{2,1,0:T(8,128)}, u32[]{:S(2)}) copy-start(s32[1,8,8]{2,1,0:T(8,128)} %param.15) | copy-start | bytes 772
  39.7 61.6 %all-to-all-start.2 = ((bf16[128,64,128]{2,1,0:T(8,128)(2,1)}), bf16[128,64,128]{2,1,0:T(8,128)(2,1)}, u32[]{:S(2)}, u32[]{:S(2)}) async-start(bf16[128,64,128]{2,1,0:T(8,128)(2,1)} %broadcast_select_fusion), calls=%async_computation.2 | async-start | bytes 4194304 | tf_op jit(solution)/shard_map/all_to_all | solution.py:110
  107.3 1.0 copy-start.1
  110.4 1.4 copy-start.2
  111.7 1.0 copy-start.1
  114.8 1.4 copy-start.2
  116.1 1.0 copy-start.1
  119.2 1.4 copy-start.2
  120.5 1.0 copy-start.1
  123.6 1.4 copy-start.2
  126.3 18.9 %copy-start.5 = (f32[1024]{0:T(1024)S(1)}, f32[1024]{0:T(1024)}, u32[]{:S(2)}) copy-start(f32[1024]{0:T(1024)} %param.14) | copy-start | bytes 12292
  144.9 1.2 copy-start.6
where the time goes:
time: 148 us
  waiting for transfers between devices  56.8 us (38%)
  starting transfers between devices  24.4 us (16%)
  blocking collectives  22.2 us (15%)
  local copies, waits for them, and re-layouts  19.1 us (13%)
  other arithmetic  14.4 us (10%)
  matrix products  10.4 us (7%)
    all_to_all x1, waiting for transfers between devices, per_device(): lax.all_to_all(outgoing, KV, split_axis=0, concat_axis=0, tiled=True)  49.2 us
    all_to_all x1, blocking collectives, from_everyone(): return lax.all_to_all(copies, axis, split_axis=0, concat_axis=0, tiled=True)  18.5 us
    all_to_all x1, starting transfers between devices, turned_blocks(): whole = lax.all_to_all(whole, axes[k], k, k, tiled=True)  16.6 us
    all_to_all x1, starting transfers between devices, per_device(): lax.all_to_all(outgoing, KV, split_axis=0, concat_axis=0, tiled=True)  7.82 us
    all_to_all x1, waiting for transfers between devices, turned_blocks(): whole = lax.all_to_all(whole, axes[k], k, k, tiled=True)  7.6 us
    dynamic_slice x8, local copies, waits for them, and re-layouts, per_device(): lax.map(attend, (queries.reshape(pair_count, 2, BLK, head_count, HD), sel...  4.53 us
    all_to_all x1, blocking collectives, turned_blocks(): whole = lax.all_to_all(whole, axes[k], k, k, tiled=True)  3.7 us
    concatenate x1, other arithmetic, per_device(): pool_pairs = jnp.concatenate([arrived, local_pairs], axis=0)  3.64 us
  transfers between devices with their start and end apart: 2, of which 2 were waited for; matrix products, arithmetic and copies ran while one was open for 5% of the time, Pallas kernels for 0%

commit v1 on v0

v1 whole, which is shorter than its diff:
```python
import functools

import jax
import jax.numpy as jnp
from jax import lax
from jax.experimental import pallas as pl
from jax.experimental.pallas import tpu as pltpu
from jax.sharding import Mesh
from jax.sharding import PartitionSpec as P

HQ = 16
HD = 64
BLK = 64
SEL = 8
HALF = BLK // 2
CORES = 2
KV = ("kv_0", "kv_1", "kv_2")
MESH = pl.DeviceIdType.MESH

rope_base = 500000.0
norm_eps = 1e-06


def rope_tables(positions):
    half_size = HD // 2
    frequency = rope_base ** (-jnp.arange(half_size, dtype=jnp.float32) / half_size)
    angles = positions.astype(jnp.float32)[:, None] * frequency[None, :]
    return jnp.cos(angles)[:, None, :], jnp.sin(angles)[:, None, :]


def rotate(vectors, cosine, sine_wave):
    half_size = HD // 2
    lower_half = vectors[..., :half_size]
    upper_half = vectors[..., half_size:]
    return jnp.concatenate(
        [
            lower_half * cosine - upper_half * sine_wave,
            upper_half * cosine + lower_half * sine_wave,
        ],
        axis=-1,
    )


def exchange_kernel(
    nz, ny, chosen_ref, pairs_ref, ra_ref, rb_ref,
    ga, gb, sa, sb, want, wall, wsm,
    want_send, want_recv, smem_sem, own_sem, ring_send, ring_recv,
    a_send, a_recv, b_send, b_recv,
):
    z, y, c = lax.axis_index("kv_0"), lax.axis_index("kv_1"), lax.axis_index("kv_2")
    rows, cols = ny * CORES, nz * CORES
    row_me, col_me = y * CORES + c, z * CORES + c
    blocks = pairs_ref.shape[1]
    me = z * rows + row_me

    lane = lax.broadcasted_iota(jnp.int32, (blocks, 128), 1)
    found = jnp.full((blocks, 128), -1, jnp.int32)
    for s in range(SEL):
        ids = jnp.broadcast_to(chosen_ref[:, s : s + 1], (blocks, 128))
        hit = (ids // blocks == lane) & (ids >= 0) & (lane != me)
        found = jnp.maximum(found, jnp.where(hit, ids % blocks, -1))
    want[...] = jnp.max(found, axis=0, keepdims=True)

    def row_peer(d):
        p = lax.rem(row_me + d, rows)
        return p, {"kv_0": z, "kv_1": p // CORES, "kv_2": lax.rem(p, CORES)}

    def col_peer(d):
        p = lax.rem(col_me + d, cols)
        return p, {"kv_0": p // CORES, "kv_1": y, "kv_2": lax.rem(p, CORES)}

    barrier = pltpu.get_barrier_semaphore()

    @pl.loop(1, rows)
    def _(d):
        _, peer = row_peer(d)
        pl.semaphore_signal(barrier, inc=1, device_id=peer, device_id_type=MESH)

    @pl.loop(1, nz)
    def _(d):
        for core in range(CORES):
            peer = {"kv_0": lax.rem(z + d, nz), "kv_1": y, "kv_2": core}
            pl.semaphore_signal(barrier, inc=1, device_id=peer, device_id_type=MESH)

    pl.semaphore_wait(barrier, rows - 1 + (nz - 1) * CORES)

    own_a = pltpu.make_async_copy(pairs_ref.at[0], ga.at[z], own_sem.at[0])
    own_b = pltpu.make_async_copy(pairs_ref.at[1], gb.at[y], own_sem.at[1])
    own_a.start()
    own_b.start()
    pltpu.make_async_copy(want, wall.at[row_me], want_recv).start()
    pltpu.make_async_copy(want, wall.at[rows + col_me], want_recv).start()

    @pl.loop(1, rows)
    def _(d):
        _, peer = row_peer(d)
        pltpu.make_async_remote_copy(
            want, wall.at[row_me], want_send, want_recv, device_id=peer, device_id_type=MESH
        ).start()

    @pl.loop(1, cols)
    def _(d):
        _, peer = col_peer(d)
        pltpu.make_async_remote_copy(
            want, wall.at[rows + col_me], want_send, want_recv, device_id=peer, device_id_type=MESH
        ).start()

    def ring_copy(axis, way, step):
        name, place, size, held = (("kv_0", z, nz, ga), ("kv_1", y, ny, gb))[axis]
        if way == 0:
            source, target = lax.rem(place - step + size, size), lax.rem(place + 1, size)
        else:
            source, target = lax.rem(place + step, size), lax.rem(place + size - 1, size)
        return pltpu.make_async_remote_copy(
            pairs_ref.at[axis] if step == 0 else held.at[source],
            held.at[source],
            ring_send.at[axis, way, step],
            ring_recv.at[axis, way, step],
            device_id={name: target},
            device_id_type=MESH,
        )

    hops = {}
    for step in range(max(nz, ny) // 2 + 1):
        for axis, size in ((0, nz), (1, ny)):
            for way, count in ((0, size // 2), (1, (size - 1) // 2)):
                if 0 < step <= count:
                    hops[axis, way, step - 1].wait_recv()
                if step < count:
                    hops[axis, way, step] = ring_copy(axis, way, step)
                    hops[axis, way, step].start()
    own_a.wait()
    own_b.wait()

    pltpu.make_async_copy(wall, wall, want_recv).wait()
    to_smem = pltpu.make_async_copy(wall, wsm, smem_sem)
    to_smem.start()
    to_smem.wait()

    @pl.loop(0, rows)
    def _(p):
        for k in range(nz):
            block = jnp.maximum(wsm[p, 0, k * rows + row_me], 0)
            sa[p, k] = ga[k, block]

    @pl.loop(0, cols)
    def _(p):
        for k in range(ny):
            block = jnp.maximum(wsm[rows + p, 0, z * rows + k * CORES + c], 0)
            sb[p, k] = gb[k, block]

    keep_a = pltpu.make_async_copy(sa.at[row_me], ra_ref.at[row_me], a_recv.at[row_me])
    keep_b = pltpu.make_async_copy(sb.at[col_me], rb_ref.at[col_me], b_recv.at[col_me])
    keep_a.start()
    keep_b.start()

    def send_a(d):
        p, peer = row_peer(d)
        return pltpu.make_async_remote_copy(
            sa.at[p], ra_ref.at[row_me], a_send.at[p], a_recv.at[row_me],
            device_id=peer, device_id_type=MESH,
        )

    def send_b(d):
        p, peer = col_peer(d)
        copy = pltpu.make_async_remote_copy(
            sb.at[p], rb_ref.at[col_me], b_send.at[p], b_recv.at[col_me],
            device_id=peer, device_id_type=MESH,
        )
        return p // CORES >= z, copy

    @pl.loop(1, max(rows, cols))
    def _(d):
        if rows == cols:
            send_a(d).start()
        else:
            @pl.when(d < rows)
            def _():
                send_a(d).start()

        @pl.when(d < cols)
        def _():
            later, copy = send_b(d)

            @pl.when(later)
            def _():
                copy.start()

    for copy in hops.values():
        copy.wait_send()
    sends = wall.at[pl.ds(0, rows + cols - 2)]
    pltpu.make_async_copy(sends, sends, want_send).wait()

    @pl.loop(1, rows)
    def _(d):
        send_a(d).wait_send()

    @pl.loop(1, cols)
    def _(d):
        later, copy = send_b(d)

        @pl.when(later)
        def _():
            copy.wait_send()

    @pl.loop(0, rows)
    def _(p):
        pltpu.make_async_copy(sa.at[p], ra_ref.at[p], a_recv.at[p]).wait()

    @pl.loop(0, cols)
    def _(p):
        @pl.when(p // CORES <= z)
        def _():
            pltpu.make_async_copy(sb.at[p], rb_ref.at[p], b_recv.at[p]).wait()


def exchange(nz, ny, chosen, pairs):
    blocks = pairs.shape[1]
    rows, cols = ny * CORES, nz * CORES
    piece = (HALF, 2 * HD)
    vmem = pl.BlockSpec(memory_space=pltpu.VMEM)
    dma = pltpu.SemaphoreType.DMA
    return pl.pallas_call(
        functools.partial(exchange_kernel, nz, ny),
        out_shape=(
            jax.ShapeDtypeStruct((rows, nz, *piece), jnp.bfloat16),
            jax.ShapeDtypeStruct((cols, ny, *piece), jnp.bfloat16),
        ),
        in_specs=[vmem, vmem],
        out_specs=(vmem, vmem),
        scratch_shapes=[
            pltpu.VMEM((nz, blocks, *piece), jnp.bfloat16),
            pltpu.VMEM((ny, blocks, *piece), jnp.bfloat16),
            pltpu.VMEM((rows, nz, *piece), jnp.bfloat16),
            pltpu.VMEM((cols, ny, *piece), jnp.bfloat16),
            pltpu.VMEM((1, 128), jnp.int32),
            pltpu.VMEM((rows + cols, 1, 128), jnp.int32),
            pltpu.SMEM((rows + cols, 1, 128), jnp.int32),
            dma, dma, dma,
            dma((2,)),
            dma((2, 2, max(nz, ny) // 2)),
            dma((2, 2, max(nz, ny) // 2)),
            dma((rows,)),
            dma((rows,)),
            dma((cols,)),
            dma((cols,)),
        ],
        compiler_params=pltpu.CompilerParams(collective_id=0, has_side_effects=True),
    )(chosen, pairs)


def attend_kernel(
    nz, ny, nt, chosen_ref, q_ref, pairs_ref, ra_ref, rb_ref, w_ref, gain_ref, out_ref,
    kv, full, scaled_w, send_sem, recv_sem,
):
    z, y, c = lax.axis_index("kv_0"), lax.axis_index("kv_1"), lax.axis_index("kv_2")
    t = lax.axis_index("tp")
    rows = ny * CORES
    me = z * rows + y * CORES + c
    blocks = pairs_ref.shape[1]
    heads, row_count = q_ref.shape[0], q_ref.shape[1]
    chunk_blocks = 2
    chunks = blocks // chunk_blocks
    chunk_rows = chunk_blocks * BLK

    barrier = pltpu.get_barrier_semaphore()
    right, left = lax.rem(t + 1, nt), lax.rem(t + nt - 1, nt)
    across = lax.rem(t + 2, nt)
    for peer in (right, left):
        pl.semaphore_signal(barrier, inc=1, device_id={"tp": peer}, device_id_type=MESH)

    lane = lax.broadcasted_iota(jnp.int32, (1, SEL * BLK), 1)
    query_row = lax.broadcasted_iota(jnp.int32, (BLK, SEL * BLK), 0)
    key_col = lax.broadcasted_iota(jnp.int32, (BLK, SEL * BLK), 1)
    causal = jnp.where((key_col < BLK) & (key_col > query_row), -jnp.inf, 0.0).astype(jnp.float32)
    value_side = lax.broadcasted_iota(jnp.int32, (1, 2 * HD), 1) >= HD
    scaled_w[...] = (w_ref[...].astype(jnp.float32) * gain_ref[...]).astype(jnp.bfloat16)

    def attend_block(b):
        bias = jnp.zeros((1, SEL * BLK), jnp.float32)
        for s in range(SEL):
            named = chosen_ref[b, s]
            owner = lax.shift_right_arithmetic(named, 3)
            index = lax.bitwise_and(named, blocks - 1)
            here = (named < 0) | (owner == me)
            owner = jnp.where(here, me, owner)
            oz, oy, oc = owner // rows, lax.rem(owner, rows) // CORES, lax.rem(owner, CORES)
            kv[pl.ds(s * BLK, HALF)] = jnp.where(
                here, pairs_ref[0, index], ra_ref[oy * CORES + oc, oz]
            )
            kv[pl.ds(s * BLK + HALF, HALF)] = jnp.where(
                here, pairs_ref[1, index], rb_ref[oz * CORES + oc, oy]
            )
            if s > 0:
                bias = jnp.where((lane // BLK == s) & (named < 0), -jnp.inf, bias)
        keys = kv[...]
        first = b * BLK if isinstance(b, int) else pl.multiple_of(b * BLK, BLK)
        query = q_ref[:, pl.ds(first, BLK), :].reshape(heads * BLK, 2 * HD)
        scores = lax.dot_general(
            query, keys, (((1,), (1,)), ((), ())), preferred_element_type=jnp.float32
        )
        scores = scores.reshape(heads, BLK, SEL * BLK) + (causal + bias)[None]
        scores = scores.reshape(heads * BLK, SEL * BLK)
        peak = jnp.max(scores, axis=1, keepdims=True)
        weights = jnp.exp(scores - peak).astype(jnp.bfloat16)
        ones_or_values = jnp.where(value_side, keys, jnp.ones((), jnp.bfloat16))
        mixed = jnp.dot(weights, ones_or_values, preferred_element_type=jnp.float32)
        turned = pltpu.roll(mixed, HD, 1)
        outs = []
        for h in range(0, heads, 2):
            lo = slice(h * BLK, (h + 1) * BLK)
            hi = slice((h + 1) * BLK, (h + 2) * BLK)
            outs.append(
                jnp.where(value_side, mixed[hi], turned[lo])
                / jnp.where(value_side, turned[hi], mixed[lo])
            )
        return jnp.concatenate(outs, axis=1).astype(jnp.bfloat16)

    def piece(owner, k):
        return full.at[owner, pl.ds(k * chunk_rows, chunk_rows)]

    def near(way, k):
        return pltpu.make_async_remote_copy(
            piece(t, k), piece(t, k), send_sem.at[way, k], recv_sem.at[way, k],
            device_id={"tp": (right, left)[way]}, device_id_type=MESH,
        )

    def onward(k):
        way = k % 2
        source = (left, right)[way]
        return pltpu.make_async_remote_copy(
            piece(source, k), piece(source, k), send_sem.at[2, k], recv_sem.at[2, k],
            device_id={"tp": (right, left)[way]}, device_id_type=MESH,
        )

    for k in range(chunks):
        for i in range(chunk_blocks):
            b = k * chunk_blocks + i
            full[t, pl.ds(b * BLK, BLK)] = attend_block(b)
        if k == 0:
            pl.semaphore_wait(barrier, 2)
        near(0, k).start()
        near(1, k).start()
        if k > 0:
            near((k - 1) % 2, k - 1).wait_recv()
            onward(k - 1).start()
    near((chunks - 1) % 2, chunks - 1).wait_recv()
    onward(chunks - 1).start()

    width = heads * HD
    for k in range(chunks):
        near((k + 1) % 2, k).wait_recv()
        onward(k).wait_recv()
        total = None
        squares = None
        for owner in range(nt):
            part = full[owner, pl.ds(k * chunk_rows, chunk_rows)]
            wide = part.astype(jnp.float32)
            square = jnp.sum(wide * wide, axis=1, keepdims=True)
            term = jnp.dot(
                part,
                scaled_w[pl.ds(owner * width, width), :],
                preferred_element_type=jnp.float32,
            )
            total = term if total is None else total + term
            squares = square if squares is None else squares + square
        inverse = lax.rsqrt(squares / (HQ * HD) + norm_eps)
        out_ref[pl.ds(k * chunk_rows, chunk_rows), :] = (inverse * total).astype(jnp.bfloat16)
    for k in range(chunks):
        near(0, k).wait_send()
        near(1, k).wait_send()
        onward(k).wait_send()


def attend(nz, ny, nt, chosen, queries, pairs, ra, rb, w_out, gain):
    heads, row_count = queries.shape[:2]
    vmem = pl.BlockSpec(memory_space=pltpu.VMEM)
    chunks = pairs.shape[1] // 2
    return pl.pallas_call(
        functools.partial(attend_kernel, nz, ny, nt),
        out_shape=jax.ShapeDtypeStruct((row_count, w_out.shape[1]), jnp.bfloat16),
        in_specs=[pl.BlockSpec(memory_space=pltpu.SMEM)] + [vmem] * 6,
        out_specs=vmem,
        scratch_shapes=[
            pltpu.VMEM((SEL * BLK, 2 * HD), jnp.bfloat16),
            pltpu.VMEM((nt, row_count, heads * HD), jnp.bfloat16),
            pltpu.VMEM(w_out.shape, jnp.bfloat16),
            pltpu.SemaphoreType.DMA((3, chunks)),
            pltpu.SemaphoreType.DMA((3, chunks)),
        ],
        compiler_params=pltpu.CompilerParams(collective_id=1, has_side_effects=True),
    )(chosen, queries, pairs, ra, rb, w_out, gain)


def per_device(tokens, w_query, w_key, w_value, w_out, out_gain, chosen):
    nz, ny, nt = lax.axis_size("kv_0"), lax.axis_size("kv_1"), lax.axis_size("tp")
    kv_place = lax.axis_index(KV)
    row_count = tokens.shape[0]
    block_count = row_count // BLK
    head_count = w_query.shape[1] // HD
    positions = kv_place * row_count + jnp.arange(row_count, dtype=jnp.int32)
    cosine, sine_wave = rope_tables(positions)
    w_pair = jnp.concatenate([w_key, w_value], axis=1)
    pair = jnp.dot(tokens, w_pair, preferred_element_type=jnp.float32)
    key_rows = rotate(pair[:, None, :HD], cosine, sine_wave)[:, 0]
    pairs = jnp.concatenate([key_rows, pair[:, HD:]], axis=1).astype(jnp.bfloat16)
    pairs = pairs.reshape(block_count, 2, HALF, 2 * HD).transpose(1, 0, 2, 3)
    chosen_ids = chosen[0]
    ra, rb = exchange(nz, ny, chosen_ids, pairs)
    queries = rotate(
        jnp.dot(tokens, w_query, preferred_element_type=jnp.float32).reshape(
            row_count, head_count, HD
        ),
        cosine,
        sine_wave,
    ).astype(jnp.bfloat16) * jnp.bfloat16(HD ** (-0.5))
    queries = jnp.pad(queries.transpose(1, 0, 2), ((0, 0), (0, 0), (0, HD)))
    return attend(nz, ny, nt, chosen_ids, queries, pairs, ra, rb, w_out, out_gain[:, None])


def solution(mesh):
    count = mesh.shape["kv"]
    ny = 8 if count == 128 else 2
    nz = count // (ny * CORES)
    finer = Mesh(
        mesh.devices.reshape(nz, ny, CORES, mesh.shape["tp"]), ("kv_0", "kv_1", "kv_2", "tp")
    )
    placed = (
        P(KV, None),
        P(None, "tp"),
        P(None, "tp"),
        P(None, "tp"),
        P(None, "tp"),
        P(),
        P("tp", KV, None),
    )
    return jax.shard_map(
        per_device, mesh=finer, in_specs=placed, out_specs=P(KV, "tp"), check_vma=False
    )
```

time: 148 us -> 94 us (0.64)
  the two profiles are of different devices: /device:TPU:8 before, /device:TPU:4 now
where the time goes in v1:
time: 94 us; the launch traced here: 93.7 us
  Pallas kernels  77.6 us (83%)
  local copies, waits for them, and re-layouts  8.45 us (9%)
  other arithmetic  4.74 us (5%)
  matrix products  2.8 us (3%)
    pallas_call x1, Pallas kernels, exchange(): pl.pallas_call(functools.partial(exchange_kernel, nz, ny), out_shape=(jax...  56.4 us
    pallas_call x1, Pallas kernels, attend(): pl.pallas_call(functools.partial(attend_kernel, nz, ny, nt), out_shape=ja...  21.2 us
    unnamed x11, local copies, waits for them, and re-layouts  5.43 us
    dot_general x1, matrix products, per_device(): jnp.dot(tokens, w_query, preferred_element_type=jnp.float32)  1.98 us

profile of v1, /device:TPU:4, one launch (start us, length us, event | category | flops | bytes accessed | tf_op | source)
XLA Modules:
  0.0 93.7 jit_solution(17987939600944770999)
XLA Ops:
  0.0 0.0 copy-start
  0.0 1.8 %multiply_cosine_fusion = (f32[512,32]{1,0:T(8,128)S(1)}, f32[512,32]{1,0:T(8,128)}) fusion(f32[32]{0:T(128)S(1)} %multiply_power_fusion, f32[512]{0:T(512)S(1)} %add_convert_fusion.1), kind=kLoop, calls=%fused_computation.9 | loop fusion | flops 16384 | bytes 133248 | tf_op jit(solution)/shard_map/cos | solution.py:28
  1.8 0.0 copy-done
  1.8 2.0 %fusion.14 = f32[512,256]{0,1:T(8,128)S(1)} fusion(bf16[512,2048]{1,0:T(8,128)(2,1)S(1)} %copy-done, bf16[2048,256]{1,0:T(8,128)(2,1)} %param.8), kind=kOutput, calls=%fused_computation.29 | convolution fusion | flops 536870912 | bytes 3670016 | tf_op jit(solution)/shard_map/dot_general | solution.py:411
  3.8 0.8 fusion.13
  4.6 1.3 %copy.16 = f32[512,4,32]{2,0,1:T(8,128)S(1)} copy(f32[512,4,32]{0,2,1:T(8,128)} %get-tuple-element.12) | data formatting | bytes 524288
  5.9 2.3 %copy.17 = f32[512,4,32]{2,0,1:T(8,128)} copy(f32[512,4,32]{0,2,1:T(8,128)} %get-tuple-element.11) | data formatting | bytes 524288
  8.1 1.5 %subtract_convert_fusion = (bf16[512,4,32]{2,0,1:T(8,128)(2,1)S(1)}, bf16[512,4,32]{2,0,1:T(8,128)(2,1)S(1)}) fusion(f32[512,4,32]{2,0,1:T(8,128)} %copy.17, f32[512,4,32]{2,0,1:T(8,128)S(1)} %copy.16, f32[512,32]{1,0:T(8,128)} %get-tuple-element.16, f32[512,32]{1,0:T(8,128)S(1)} %get-tuple-element.15), kind=kLoop, calls=%fused_computation.2 | loop fusion | flops 524288 | bytes 917504 | tf_op jit(solution)/shard_map/convert.7
  9.7 0.0 copy-start.1
  9.7 0.0 copy-start.2
  9.7 0.3 fusion
  10.0 0.9 pad.4.q_ref
  10.9 0.0 copy-done.1
  10.9 0.0 copy-done.2
  11.0 0.0 copy-start.3
  11.0 0.8 convolution_bitcast_fusion
  11.8 0.3 fusion.9
  12.1 0.1 copy.10
  12.3 0.1 copy.11
  12.4 0.8 copy_bitcast_fusion.pairs_ref
  13.2 56.4 %shard_map.73 = (bf16[16,8,32,128]{3,2,1,0:T(8,128)(2,1)}, bf16[16,8,32,128]{3,2,1,0:T(8,128)(2,1)}) custom-call(s32[8,8]{1,0:T(8,128)} %bitcast.19, bf16[2,8,32,128]{3,2,1,0:T(8,128)(2,1)} %copy_bitcast_fusion.pairs_ref), custom_call_target="tpu_custom_call" | custom-call | tf_op jit(solution)/shard_map/pallas_call | solution.py:223
  69.6 0.0 copy-done.3
  69.6 1.0 %copy.14.gain_ref = f32[1024,1]{1,0:T(8,128)} copy(f32[1024,1]{0,1:T(1,128)S(1)} %bitcast.21) | data formatting | bytes 8192 | tf_op jit(solution)/shard_map/broadcast_in_dim | solution.py:418
  70.7 21.2 %shard_map.74 = bf16[512,512]{1,0:T(8,128)(2,1)} custom-call(s32[8,8]{1,0:T(8,128)} %bitcast.20, bf16[4,512,128]{2,1,0:T(8,128)(2,1)} %pad.4.q_ref, bf16[2,8,32,128]{3,2,1,0:T(8,128)(2,1)} %copy_bitcast_fusion.pairs_ref, bf16[16,8,32,128]{3,2,1,0:T(8,128)(2,1)} %get-tuple-element.7.ra_ref, bf16[16,8,32,128]{3,2,1,0:T(8,128)(2,1)} %get-tuple-element.8.rb_ref, ...), custom_call_target="tpu_custom_call" | custom-call | tf_op jit(solution)/shard_map/pallas_call | solution.py:379
  91.8 1.9 %copy.20 = bf16[512,512]{1,0:T(8,128)(2,1)} copy(bf16[512,512]{1,0:T(8,128)(2,1)} %shard_map.74) | data formatting | bytes 1048576
  (5 shorter events, 0.0 us)
Async XLA Ops:
  0.0 1.8 %copy-start = (bf16[512,2048]{1,0:T(8,128)(2,1)S(1)}, bf16[512,2048]{1,0:T(8,128)(2,1)}, u32[]{:S(2)}) copy-start(bf16[512,2048]{1,0:T(8,128)(2,1)} %param.7) | copy-start | bytes 6291460
  9.7 1.3 %copy-start.1 = (bf16[2048,64]{0,1:T(8,128)(2,1)S(1)}, bf16[2048,64]{0,1:T(8,128)(2,1)}, u32[]{:S(2)}) copy-start(bf16[2048,64]{0,1:T(8,128)(2,1)} %param.10) | copy-start | bytes 786436
  9.7 1.3 %copy-start.2 = (bf16[2048,64]{0,1:T(8,128)(2,1)S(1)}, bf16[2048,64]{0,1:T(8,128)(2,1)}, u32[]{:S(2)}) copy-start(bf16[2048,64]{0,1:T(8,128)(2,1)} %param.9) | copy-start | bytes 786436
  11.0 58.6 %copy-start.3 = (f32[1024]{0:T(1024)S(1)}, f32[1024]{0:T(1024)}, u32[]{:S(2)}) copy-start(f32[1024]{0:T(1024)} %param.12) | copy-start | bytes 12292

commit v2 on v1

v2 whole, which is shorter than its diff:
```python
import functools

import jax
import jax.numpy as jnp
from jax import lax
from jax.experimental import pallas as pl
from jax.experimental.pallas import tpu as pltpu
from jax.sharding import Mesh
from jax.sharding import PartitionSpec as P

HQ = 16
HD = 64
BLK = 64
SEL = 8
HALF = BLK // 2
CORES = 2
KV = ("kv_0", "kv_1", "kv_2")
MESH = pl.DeviceIdType.MESH

rope_base = 500000.0
norm_eps = 1e-06


def layer_kernel(
    nz, ny, nt,
    ids_ref, chosen_ref, table_ref, gain_ref, tokens_hbm, wk_hbm, wv_hbm, wq_hbm, wo_hbm, out_ref,
    tokens, w_pair, w_query, w_out, pairs, query, ga, gb, sa, sb, ra, rb, want, wall, wsm, kv, full,
    load_sem, want_send, want_recv, smem_sem, ring_send, ring_recv,
    a_send, a_recv, b_send, b_recv, tp_send, tp_recv,
):
    z, y, c = lax.axis_index("kv_0"), lax.axis_index("kv_1"), lax.axis_index("kv_2")
    t = lax.axis_index("tp")
    rows, cols = ny * CORES, nz * CORES
    row_me, col_me = y * CORES + c, z * CORES + c
    blocks = pairs.shape[1]
    me = z * rows + row_me
    heads = query.shape[0]

    def row_peer(d):
        p = lax.rem(row_me + d, rows)
        return p, {"kv_0": z, "kv_1": p // CORES, "kv_2": lax.rem(p, CORES)}

    def col_peer(d):
        p = lax.rem(col_me + d, cols)
        return p, {"kv_0": p // CORES, "kv_1": y, "kv_2": lax.rem(p, CORES)}

    right, left = lax.rem(t + 1, nt), lax.rem(t + nt - 1, nt)
    barrier = pltpu.get_barrier_semaphore()

    @pl.loop(1, rows)
    def _(d):
        _, peer = row_peer(d)
        pl.semaphore_signal(barrier, inc=1, device_id=peer, device_id_type=MESH)

    @pl.loop(1, nz)
    def _(d):
        for core in range(CORES):
            peer = {"kv_0": lax.rem(z + d, nz), "kv_1": y, "kv_2": core}
            pl.semaphore_signal(barrier, inc=1, device_id=peer, device_id_type=MESH)

    for peer in (right, left):
        pl.semaphore_signal(barrier, inc=1, device_id={"tp": peer}, device_id_type=MESH)

    loads = [
        pltpu.make_async_copy(wk_hbm, w_pair.at[pl.ds(0, HD)], load_sem.at[0]),
        pltpu.make_async_copy(wv_hbm, w_pair.at[pl.ds(HD, HD)], load_sem.at[1]),
        pltpu.make_async_copy(tokens_hbm, tokens, load_sem.at[2]),
        pltpu.make_async_copy(wq_hbm, w_query, load_sem.at[3]),
        pltpu.make_async_copy(wo_hbm, w_out, load_sem.at[4]),
    ]
    for load in loads:
        load.start()

    lane = lax.broadcasted_iota(jnp.int32, (blocks, 128), 1)
    found = jnp.full((blocks, 128), -1, jnp.int32)
    for s in range(SEL):
        ids = jnp.broadcast_to(ids_ref[:, s : s + 1], (blocks, 128))
        hit = (ids // blocks == lane) & (ids >= 0) & (lane != me)
        found = jnp.maximum(found, jnp.where(hit, ids % blocks, -1))
    want[...] = jnp.max(found, axis=0, keepdims=True)

    head_lane = lax.broadcasted_iota(jnp.int32, (1, 2 * HD), 1)
    value_side = head_lane >= HD
    lower_side = head_lane % HD < HD // 2

    def turned(wide, b, only_keys):
        cos_row, sin_row = table_ref[0, pl.ds(0, BLK)], table_ref[1, pl.ds(0, BLK)]
        cos_base, sin_base = table_ref[0, pl.ds(BLK + b, 1)], table_ref[1, pl.ds(BLK + b, 1)]
        cosine = cos_base * cos_row - sin_base * sin_row
        sine_wave = sin_base * cos_row + cos_base * sin_row
        if only_keys:
            cosine = jnp.where(value_side, 1.0, cosine)
            sine_wave = jnp.where(value_side, 0.0, sine_wave)
        other = jnp.where(lower_side, pltpu.roll(wide, 3 * HD // 2, 1), pltpu.roll(wide, HD // 2, 1))
        return wide * cosine + other * sine_wave

    for load in loads[:3]:
        load.wait()
    pair = lax.dot_general(
        tokens[...], w_pair[...], (((1,), (1,)), ((), ())), preferred_element_type=jnp.float32
    )
    for b in range(blocks):
        held = turned(pair[b * BLK : (b + 1) * BLK], b, True).astype(jnp.bfloat16)
        pairs[0, b] = held[:HALF]
        pairs[1, b] = held[HALF:]

    pl.semaphore_wait(barrier, rows - 1 + (nz - 1) * CORES + 2)

    pltpu.make_async_copy(want, wall.at[row_me], want_recv).start()
    pltpu.make_async_copy(want, wall.at[rows + col_me], want_recv).start()

    @pl.loop(1, rows)
    def _(d):
        _, peer = row_peer(d)
        pltpu.make_async_remote_copy(
            want, wall.at[row_me], want_send, want_recv, device_id=peer, device_id_type=MESH
        ).start()

    @pl.loop(1, cols)
    def _(d):
        _, peer = col_peer(d)
        pltpu.make_async_remote_copy(
            want, wall.at[rows + col_me], want_send, want_recv, device_id=peer, device_id_type=MESH
        ).start()

    def ring_copy(axis, way, step):
        name, place, size, held = (("kv_0", z, nz, ga), ("kv_1", y, ny, gb))[axis]
        target = lax.rem(place + (1, size - 1)[way], size)
        return pltpu.make_async_remote_copy(
            pairs.at[axis] if step == 0 else held[2 * step - 2 + way],
            held[2 * step + way],
            ring_send.at[axis, way, step],
            ring_recv.at[axis, way, step],
            device_id={name: target},
            device_id_type=MESH,
        )

    def source_of(place, size, k):
        if k % 2:
            return lax.rem(place - (k + 1) // 2 + size, size)
        return lax.rem(place + k // 2, size)

    def groups_of(size):
        found = [(0, 1)]
        for s in range(1, size // 2 + 1):
            found.append((2 * s - 1, min(2 * s + 1, size)))
        if size >= 8:
            found[-2:] = [(found[-2][0], found[-1][1])]
        return found

    def ready_at(size, group):
        return group[1] // 2

    groups_a, groups_b = groups_of(nz), groups_of(ny)

    def send_a(d, g):
        p, peer = row_peer(d)
        lo, hi = groups_a[g]
        part = pl.ds(lo, hi - lo)
        return pltpu.make_async_remote_copy(
            sa.at[p, part], ra.at[row_me, part], a_send.at[g, p], a_recv.at[g, row_me],
            device_id=peer, device_id_type=MESH,
        )

    def send_b(d, g):
        p, peer = col_peer(d)
        lo, hi = groups_b[g]
        part = pl.ds(lo, hi - lo)
        copy = pltpu.make_async_remote_copy(
            sb.at[p, part], rb.at[col_me, part], b_send.at[g, p], b_recv.at[g, col_me],
            device_id=peer, device_id_type=MESH,
        )
        return p // CORES >= z, copy

    def needed_a(g):
        return z >= (groups_a[g][0] + 1) // 2

    def select_a(g):
        @pl.when(needed_a(g))
        def _():
            @pl.loop(0, rows)
            def _(p):
                for k in range(*groups_a[g]):
                    source = source_of(z, nz, k)
                    block = jnp.maximum(wsm[p, 0, source * rows + row_me], 0)
                    sa[p, k] = pairs[0, block] if k == 0 else ga[k - 1][block]

    def select_b(g):
        @pl.loop(0, cols)
        def _(p):
            for k in range(*groups_b[g]):
                source = source_of(y, ny, k)
                block = jnp.maximum(wsm[rows + p, 0, z * rows + source * CORES + c], 0)
                sb[p, k] = pairs[1, block] if k == 0 else gb[k - 1][block]

    def start_a(g):
        lo, hi = groups_a[g]
        part = pl.ds(lo, hi - lo)

        @pl.when(needed_a(g))
        def _():
            @pl.loop(1, rows)
            def _(d):
                send_a(d, g).start()

            pltpu.make_async_copy(
                sa.at[row_me, part], ra.at[row_me, part], a_recv.at[g, row_me]
            ).start()

    def start_b(g):
        lo, hi = groups_b[g]
        part = pl.ds(lo, hi - lo)

        @pl.loop(1, cols)
        def _(d):
            later, copy = send_b(d, g)

            @pl.when(later)
            def _():
                copy.start()

        pltpu.make_async_copy(
            sb.at[col_me, part], rb.at[col_me, part], b_recv.at[g, col_me]
        ).start()

    hops = {}
    for step in range(max(nz, ny) // 2 + 1):
        for axis, size in ((0, nz), (1, ny)):
            for way, count in ((0, size // 2), (1, (size - 1) // 2)):
                if 0 < step <= count:
                    hops[axis, way, step - 1].wait_recv()
                if step < count:
                    hops[axis, way, step] = ring_copy(axis, way, step)
                    hops[axis, way, step].start()
        if step == 0:
            loads[3].wait()
            product = jnp.dot(tokens[...], w_query[...], preferred_element_type=jnp.float32)
            for b in range(blocks):
                for h in range(0, heads, 2):
                    wide = product[b * BLK : (b + 1) * BLK, h * HD : (h + 2) * HD]
                    wide = turned(wide, b, False) * (HD ** -0.5)
                    spot = pl.ds(b * BLK, BLK)
                    query[h, spot] = jnp.where(value_side, 0.0, wide).astype(jnp.bfloat16)
                    query[h + 1, spot] = jnp.where(
                        value_side, 0.0, pltpu.roll(wide, HD, 1)
                    ).astype(jnp.bfloat16)
            pltpu.make_async_copy(wall, wall, want_recv).wait()
            to_smem = pltpu.make_async_copy(wall, wsm, smem_sem)
            to_smem.start()
            to_smem.wait()
        now_a = [g for g, group in enumerate(groups_a) if ready_at(nz, group) == step]
        now_b = [g for g, group in enumerate(groups_b) if ready_at(ny, group) == step]
        for g in now_a:
            select_a(g)
        for g in now_b:
            select_b(g)
        for g in now_a:
            start_a(g)
        for g in now_b:
            start_b(g)

    loads[4].wait()

    @pl.loop(0, rows)
    def _(p):
        for g, (lo, hi) in enumerate(groups_a):
            part = pl.ds(lo, hi - lo)

            @pl.when(needed_a(g))
            def _():
                pltpu.make_async_copy(sa.at[p, part], ra.at[p, part], a_recv.at[g, p]).wait()

    @pl.loop(0, cols)
    def _(p):
        @pl.when(p // CORES <= z)
        def _():
            for g, (lo, hi) in enumerate(groups_b):
                part = pl.ds(lo, hi - lo)
                pltpu.make_async_copy(sb.at[p, part], rb.at[p, part], b_recv.at[g, p]).wait()

    chunk_blocks = 2
    chunks = blocks // chunk_blocks
    chunk_rows = chunk_blocks * BLK
    key_lane = lax.broadcasted_iota(jnp.int32, (1, SEL * BLK), 1)
    query_row = lax.broadcasted_iota(jnp.int32, (BLK, SEL * BLK), 0)
    key_col = lax.broadcasted_iota(jnp.int32, (BLK, SEL * BLK), 1)
    causal = jnp.where((key_col < BLK) & (key_col > query_row), -jnp.inf, 0.0).astype(jnp.float32)

    def slot_of(place, size, owner):
        r = lax.rem(place - owner + size, size)
        return jnp.where(r <= size // 2, jnp.maximum(2 * r - 1, 0), 2 * (size - r))

    def attend_block(b):
        bias = jnp.zeros((1, SEL * BLK), jnp.float32)
        for s in range(SEL):
            named = chosen_ref[b, s]
            owner = lax.shift_right_arithmetic(named, 3)
            index = lax.bitwise_and(named, blocks - 1)
            here = (named < 0) | (owner == me)
            owner = jnp.where(here, me, owner)
            oz, oy, oc = owner // rows, lax.rem(owner, rows) // CORES, lax.rem(owner, CORES)
            kv[pl.ds(s * BLK, HALF)] = jnp.where(
                here, pairs[0, index], ra[oy * CORES + oc, slot_of(z, nz, oz)]
            )
            kv[pl.ds(s * BLK + HALF, HALF)] = jnp.where(
                here, pairs[1, index], rb[oz * CORES + oc, slot_of(y, ny, oy)]
            )
            if s > 0:
                bias = jnp.where((key_lane // BLK == s) & (named < 0), -jnp.inf, bias)
        keys = kv[...]
        queries = query[:, pl.ds(b * BLK, BLK), :].reshape(heads * BLK, 2 * HD)
        scores = lax.dot_general(
            queries, keys, (((1,), (1,)), ((), ())), preferred_element_type=jnp.float32
        )
        scores = scores.reshape(heads, BLK, SEL * BLK) + (causal + bias)[None]
        scores = scores.reshape(heads * BLK, SEL * BLK)
        peak = jnp.max(scores, axis=1, keepdims=True)
        weights = jnp.exp(scores - peak).astype(jnp.bfloat16)
        ones_or_values = jnp.where(value_side, keys, jnp.ones((), jnp.bfloat16))
        mixed = jnp.dot(weights, ones_or_values, preferred_element_type=jnp.float32)
        swapped = pltpu.roll(mixed, HD, 1)
        outs = []
        for h in range(0, heads, 2):
            lo = slice(h * BLK, (h + 1) * BLK)
            hi = slice((h + 1) * BLK, (h + 2) * BLK)
            outs.append(
                jnp.where(value_side, mixed[hi], swapped[lo])
                / jnp.where(value_side, swapped[hi], mixed[lo])
            )
        return jnp.concatenate(outs, axis=1).astype(jnp.bfloat16)

    def piece(owner, k):
        return full.at[owner, pl.ds(k * chunk_rows, chunk_rows)]

    def near(way, k):
        return pltpu.make_async_remote_copy(
            piece(t, k), piece(t, k), tp_send.at[way, k], tp_recv.at[way, k],
            device_id={"tp": (right, left)[way]}, device_id_type=MESH,
        )

    def onward(k):
        way = k % 2
        source = (left, right)[way]
        return pltpu.make_async_remote_copy(
            piece(source, k), piece(source, k), tp_send.at[2, k], tp_recv.at[2, k],
            device_id={"tp": (right, left)[way]}, device_id_type=MESH,
        )

    for k in range(chunks):
        for i in range(chunk_blocks):
            b = k * chunk_blocks + i
            full[t, pl.ds(b * BLK, BLK)] = attend_block(b)
        near(0, k).start()
        near(1, k).start()
        if k > 0:
            near((k - 1) % 2, k - 1).wait_recv()
            onward(k - 1).start()
    near((chunks - 1) % 2, chunks - 1).wait_recv()
    onward(chunks - 1).start()

    width = heads * HD
    for k in range(chunks):
        near((k + 1) % 2, k).wait_recv()
        onward(k).wait_recv()
        total = None
        squares = None
        for owner in range(nt):
            wide = full[owner, pl.ds(k * chunk_rows, chunk_rows)].astype(jnp.float32)
            square = jnp.sum(wide * wide, axis=1, keepdims=True)
            scaled = (wide * gain_ref[:, pl.ds(owner * width, width)]).astype(jnp.bfloat16)
            term = jnp.dot(
                scaled,
                w_out[pl.ds(owner * width, width), :],
                preferred_element_type=jnp.float32,
            )
            total = term if total is None else total + term
            squares = square if squares is None else squares + square
        inverse = lax.rsqrt(squares / (HQ * HD) + norm_eps)
        out_ref[pl.ds(k * chunk_rows, chunk_rows), :] = (inverse * total).astype(jnp.bfloat16)

    for copy in hops.values():
        copy.wait_send()
    sends = wall.at[pl.ds(0, rows + cols - 2)]
    pltpu.make_async_copy(sends, sends, want_send).wait()

    @pl.loop(1, rows)
    def _(d):
        for g in range(len(groups_a)):
            @pl.when(needed_a(g))
            def _():
                send_a(d, g).wait_send()

    @pl.loop(1, cols)
    def _(d):
        for g in range(len(groups_b)):
            later, copy = send_b(d, g)

            @pl.when(later)
            def _():
                copy.wait_send()

    for k in range(chunks):
        near(0, k).wait_send()
        near(1, k).wait_send()
        onward(k).wait_send()


def per_device(tokens, w_query, w_key, w_value, w_out, out_gain, chosen):
    nz, ny, nt = lax.axis_size("kv_0"), lax.axis_size("kv_1"), lax.axis_size("tp")
    kv_place = lax.axis_index(KV)
    row_count, depth = tokens.shape
    blocks = row_count // BLK
    heads = w_query.shape[1] // HD
    rows, cols = ny * CORES, nz * CORES
    half_size = HD // 2
    frequency = rope_base ** (-jnp.arange(half_size, dtype=jnp.float32) / half_size)
    places = jnp.concatenate(
        [
            jnp.arange(BLK, dtype=jnp.int32),
            kv_place * row_count + BLK * jnp.arange(blocks, dtype=jnp.int32),
        ]
    )
    angles = places.astype(jnp.float32)[:, None] * jnp.tile(frequency, 4)[None, :]
    sign = jnp.where(jnp.arange(2 * HD) % HD < half_size, -1.0, 1.0)
    table = jnp.stack([jnp.cos(angles), jnp.sin(angles) * sign])

    piece = (HALF, 2 * HD)
    vmem = pl.BlockSpec(memory_space=pltpu.VMEM)
    far = pl.BlockSpec(memory_space=pl.ANY)
    dma = pltpu.SemaphoreType.DMA
    bf16 = jnp.bfloat16
    steps = max(nz, ny) // 2
    return pl.pallas_call(
        functools.partial(layer_kernel, nz, ny, nt),
        out_shape=jax.ShapeDtypeStruct((row_count, w_out.shape[1]), bf16),
        in_specs=[vmem, pl.BlockSpec(memory_space=pltpu.SMEM), vmem, vmem] + [far] * 5,
        out_specs=vmem,
        scratch_shapes=[
            pltpu.VMEM((row_count, depth), bf16),
            pltpu.VMEM((2 * HD, depth), bf16),
            pltpu.VMEM(w_query.shape, bf16),
            pltpu.VMEM(w_out.shape, bf16),
            pltpu.VMEM((2, blocks, *piece), bf16),
            pltpu.VMEM((heads, row_count, 2 * HD), bf16),
            [pltpu.VMEM((blocks, *piece), bf16)] * (nz - 1),
            [pltpu.VMEM((blocks, *piece), bf16)] * (ny - 1),
            pltpu.VMEM((rows, nz, *piece), bf16),
            pltpu.VMEM((cols, ny, *piece), bf16),
            pltpu.VMEM((rows, nz, *piece), bf16),
            pltpu.VMEM((cols, ny, *piece), bf16),
            pltpu.VMEM((1, 128), jnp.int32),
            pltpu.VMEM((rows + cols, 1, 128), jnp.int32),
            pltpu.SMEM((rows + cols, 1, 128), jnp.int32),
            pltpu.VMEM((SEL * BLK, 2 * HD), bf16),
            pltpu.VMEM((nt, row_count, heads * HD), bf16),
            dma((5,)),
            dma, dma, dma,
            dma((2, 2, steps)),
            dma((2, 2, steps)),
            dma((4, rows)),
            dma((4, rows)),
            dma((4, cols)),
            dma((4, cols)),
            dma((3, blocks // 2)),
            dma((3, blocks // 2)),
        ],
        compiler_params=pltpu.CompilerParams(collective_id=0, has_side_effects=True),
    )(
        chosen[0], chosen[0], table, out_gain[None, :],
        tokens, w_key.T, w_value.T, w_query, w_out,
    )


def solution(mesh):
    count = mesh.shape["kv"]
    ny = 8 if count == 128 else 2
    nz = count // (ny * CORES)
    finer = Mesh(
        mesh.devices.reshape(nz, ny, CORES, mesh.shape["tp"]), ("kv_0", "kv_1", "kv_2", "tp")
    )
    placed = (
        P(KV, None),
        P(None, "tp"),
        P(None, "tp"),
        P(None, "tp"),
        P(None, "tp"),
        P(),
        P("tp", KV, None),
    )
    return jax.shard_map(
        per_device, mesh=finer, in_specs=placed, out_specs=P(KV, "tp"), check_vma=False
    )
```

time: 94 us -> 78.5 us (0.84)
  the two profiles are of different devices: /device:TPU:4 before, /device:TPU:196 now
where the time goes in v2:
time: 78.5 us; the launch traced here: 78.3 us
  Pallas kernels  75.4 us (96%)
  local copies, waits for them, and re-layouts  1.96 us (2%)
  other arithmetic  0.95 us (1%)
    pallas_call x1, Pallas kernels, per_device(): pl.pallas_call(functools.partial(layer_kernel, nz, ny, nt), out_shape=jax...  75.4 us
    unnamed x1, local copies, waits for them, and re-layouts  1.87 us

profile of v2, /device:TPU:196, one launch (start us, length us, event | category | flops | bytes accessed | tf_op | source)
XLA Modules:
  0.0 78.3 jit_solution(8456781809400773070)
XLA Ops:
  0.0 0.1 add_convert_fusion
  0.1 0.1 mul.60
  0.2 0.2 multiply_cosine_fusion
  0.4 0.6 pad_maximum_fusion.table_ref
  1.1 75.4 %shard_map.73 = bf16[512,512]{1,0:T(8,128)(2,1)} custom-call(s32[8,8]{1,0:T(8,128)} %bitcast.6, s32[8,8]{1,0:T(8,128)} %bitcast.7, f32[2,72,128]{2,1,0:T(8,128)} %pad_maximum_fusion.table_ref, f32[1,1024]{1,0:T(1,128)} %bitcast.8, bf16[512,2048]{1,0:T(8,128)(2,1)} %tokens_hbm.1, bf16[64,2048]{1,0:T(8,128)(2,1)} %bitcast.4, bf16[64,2048]{1,0:T(8,128)(2,1)} %bitcast.5, ...), custom_call_target="tpu_custom_call" | custom-call | tf_op jit(solution)/shard_map/pallas_call | solution.py:433
  76.5 1.9 %copy.9 = bf16[512,512]{1,0:T(8,128)(2,1)} copy(bf16[512,512]{1,0:T(8,128)(2,1)} %shard_map.73) | data formatting | bytes 1048576
  (5 shorter events, 0.0 us)

commit v3 on v2

--- a/solution.py
+++ b/solution.py
@@ -34,7 +34,7 @@
     row_me, col_me = y * CORES + c, z * CORES + c
     blocks = pairs.shape[1]
     me = z * rows + row_me
-    heads = query.shape[0]
+    heads, row_count = query.shape[0], query.shape[1]
 
     def row_peer(d):
         p = lax.rem(row_me + d, rows)
@@ -148,8 +148,8 @@
             found[-2:] = [(found[-2][0], found[-1][1])]
         return found
 
-    def ready_at(size, group):
-        return group[1] // 2
+    def sent_at(group):
+        return min(group[1] // 2 + 1, last)
 
     groups_a, groups_b = groups_of(nz), groups_of(ny)
 
@@ -224,7 +224,9 @@
         ).start()
 
     hops = {}
-    for step in range(max(nz, ny) // 2 + 1):
+    last = max(nz, ny) // 2
+
+    def ring_step(step):
         for axis, size in ((0, nz), (1, ny)):
             for way, count in ((0, size // 2), (1, (size - 1) // 2)):
                 if 0 < step <= count:
@@ -232,24 +234,18 @@
                 if step < count:
                     hops[axis, way, step] = ring_copy(axis, way, step)
                     hops[axis, way, step].start()
-        if step == 0:
-            loads[3].wait()
-            product = jnp.dot(tokens[...], w_query[...], preferred_element_type=jnp.float32)
-            for b in range(blocks):
-                for h in range(0, heads, 2):
-                    wide = product[b * BLK : (b + 1) * BLK, h * HD : (h + 2) * HD]
-                    wide = turned(wide, b, False) * (HD ** -0.5)
-                    spot = pl.ds(b * BLK, BLK)
-                    query[h, spot] = jnp.where(value_side, 0.0, wide).astype(jnp.bfloat16)
-                    query[h + 1, spot] = jnp.where(
-                        value_side, 0.0, pltpu.roll(wide, HD, 1)
-                    ).astype(jnp.bfloat16)
-            pltpu.make_async_copy(wall, wall, want_recv).wait()
-            to_smem = pltpu.make_async_copy(wall, wsm, smem_sem)
-            to_smem.start()
-            to_smem.wait()
-        now_a = [g for g, group in enumerate(groups_a) if ready_at(nz, group) == step]
-        now_b = [g for g, group in enumerate(groups_b) if ready_at(ny, group) == step]
+
+    ring_step(0)
+    ring_step(1)
+    pltpu.make_async_copy(wall, wall, want_recv).wait()
+    to_smem = pltpu.make_async_copy(wall, wsm, smem_sem)
+    to_smem.start()
+    to_smem.wait()
+    for step in range(1, last + 1):
+        if step > 1:
+            ring_step(step)
+        now_a = [g for g, group in enumerate(groups_a) if sent_at(group) == step]
+        now_b = [g for g, group in enumerate(groups_b) if sent_at(group) == step]
         for g in now_a:
             select_a(g)
         for g in now_b:
@@ -259,6 +255,17 @@
         for g in now_b:
             start_b(g)
 
+    loads[3].wait()
+    product = jnp.dot(tokens[...], w_query[...], preferred_element_type=jnp.float32)
+    for b in range(blocks):
+        for h in range(0, heads, 2):
+            wide = product[b * BLK : (b + 1) * BLK, h * HD : (h + 2) * HD]
+            wide = turned(wide, b, False) * (HD ** -0.5)
+            spot = pl.ds(b * BLK, BLK)
+            query[h, spot] = jnp.where(value_side, 0.0, wide).astype(jnp.bfloat16)
+            query[h + 1, spot] = jnp.where(
+                value_side, 0.0, pltpu.roll(wide, HD, 1)
+            ).astype(jnp.bfloat16)
     loads[4].wait()
 
     @pl.loop(0, rows)
@@ -278,9 +285,8 @@
                 part = pl.ds(lo, hi - lo)
                 pltpu.make_async_copy(sb.at[p, part], rb.at[p, part], b_recv.at[g, p]).wait()
 
-    chunk_blocks = 2
-    chunks = blocks // chunk_blocks
-    chunk_rows = chunk_blocks * BLK
+    lag = 3
+    out_rows = 2 * BLK
     key_lane = lax.broadcasted_iota(jnp.int32, (1, SEL * BLK), 1)
     query_row = lax.broadcasted_iota(jnp.int32, (BLK, SEL * BLK), 0)
     key_col = lax.broadcasted_iota(jnp.int32, (BLK, SEL * BLK), 1)
@@ -299,15 +305,15 @@
             here = (named < 0) | (owner == me)
             owner = jnp.where(here, me, owner)
             oz, oy, oc = owner // rows, lax.rem(owner, rows) // CORES, lax.rem(owner, CORES)
-            kv[pl.ds(s * BLK, HALF)] = jnp.where(
+            kv[b, pl.ds(s * BLK, HALF)] = jnp.where(
                 here, pairs[0, index], ra[oy * CORES + oc, slot_of(z, nz, oz)]
             )
-            kv[pl.ds(s * BLK + HALF, HALF)] = jnp.where(
+            kv[b, pl.ds(s * BLK + HALF, HALF)] = jnp.where(
                 here, pairs[1, index], rb[oz * CORES + oc, slot_of(y, ny, oy)]
             )
             if s > 0:
                 bias = jnp.where((key_lane // BLK == s) & (named < 0), -jnp.inf, bias)
-        keys = kv[...]
+        keys = kv[b]
         queries = query[:, pl.ds(b * BLK, BLK), :].reshape(heads * BLK, 2 * HD)
         scores = lax.dot_general(
             queries, keys, (((1,), (1,)), ((), ())), preferred_element_type=jnp.float32
@@ -330,7 +336,7 @@
         return jnp.concatenate(outs, axis=1).astype(jnp.bfloat16)
 
     def piece(owner, k):
-        return full.at[owner, pl.ds(k * chunk_rows, chunk_rows)]
+        return full.at[owner, pl.ds(k * BLK, BLK)]
 
     def near(way, k):
         return pltpu.make_async_remote_copy(
@@ -346,26 +352,28 @@
             device_id={"tp": (right, left)[way]}, device_id_type=MESH,
         )
 
-    for k in range(chunks):
-        for i in range(chunk_blocks):
-            b = k * chunk_blocks + i
-            full[t, pl.ds(b * BLK, BLK)] = attend_block(b)
-        near(0, k).start()
-        near(1, k).start()
-        if k > 0:
-            near((k - 1) % 2, k - 1).wait_recv()
-            onward(k - 1).start()
-    near((chunks - 1) % 2, chunks - 1).wait_recv()
-    onward(chunks - 1).start()
+    def pass_on(k):
+        near(k % 2, k).wait_recv()
+        onward(k).start()
+
+    for b in range(blocks):
+        full[t, pl.ds(b * BLK, BLK)] = attend_block(b)
+        near(0, b).start()
+        near(1, b).start()
+        if b >= lag:
+            pass_on(b - lag)
+    for b in range(blocks - lag, blocks):
+        pass_on(b)
 
     width = heads * HD
-    for k in range(chunks):
-        near((k + 1) % 2, k).wait_recv()
-        onward(k).wait_recv()
+    for k in range(row_count // out_rows):
+        for b in range(k * out_rows // BLK, (k + 1) * out_rows // BLK):
+            near((b + 1) % 2, b).wait_recv()
+            onward(b).wait_recv()
         total = None
         squares = None
         for owner in range(nt):
-            wide = full[owner, pl.ds(k * chunk_rows, chunk_rows)].astype(jnp.float32)
+            wide = full[owner, pl.ds(k * out_rows, out_rows)].astype(jnp.float32)
             square = jnp.sum(wide * wide, axis=1, keepdims=True)
             scaled = (wide * gain_ref[:, pl.ds(owner * width, width)]).astype(jnp.bfloat16)
             term = jnp.dot(
@@ -376,7 +384,7 @@
             total = term if total is None else total + term
             squares = square if squares is None else squares + square
         inverse = lax.rsqrt(squares / (HQ * HD) + norm_eps)
-        out_ref[pl.ds(k * chunk_rows, chunk_rows), :] = (inverse * total).astype(jnp.bfloat16)
+        out_ref[pl.ds(k * out_rows, out_rows), :] = (inverse * total).astype(jnp.bfloat16)
 
     for copy in hops.values():
         copy.wait_send()
@@ -399,7 +407,7 @@
             def _():
                 copy.wait_send()
 
-    for k in range(chunks):
+    for k in range(blocks):
         near(0, k).wait_send()
         near(1, k).wait_send()
         onward(k).wait_send()
@@ -426,7 +434,7 @@
 
     piece = (HALF, 2 * HD)
     vmem = pl.BlockSpec(memory_space=pltpu.VMEM)
-    far = pl.BlockSpec(memory_space=pl.ANY)
+    far = pl.BlockSpec(memory_space=pltpu.HBM)
     dma = pltpu.SemaphoreType.DMA
     bf16 = jnp.bfloat16
     steps = max(nz, ny) // 2
@@ -451,7 +459,7 @@
             pltpu.VMEM((1, 128), jnp.int32),
             pltpu.VMEM((rows + cols, 1, 128), jnp.int32),
             pltpu.SMEM((rows + cols, 1, 128), jnp.int32),
-            pltpu.VMEM((SEL * BLK, 2 * HD), bf16),
+            pltpu.VMEM((blocks, SEL * BLK, 2 * HD), bf16),
             pltpu.VMEM((nt, row_count, heads * HD), bf16),
             dma((5,)),
             dma, dma, dma,
@@ -461,8 +469,8 @@
             dma((4, rows)),
             dma((4, cols)),
             dma((4, cols)),
-            dma((3, blocks // 2)),
-            dma((3, blocks // 2)),
+            dma((3, blocks)),
+            dma((3, blocks)),
         ],
         compiler_params=pltpu.CompilerParams(collective_id=0, has_side_effects=True),
     )(

time: 78.5 us -> 69.6 us (0.89)
  Pallas kernels: 75.4 us -> 66.5 us
    pallas_call x1, Pallas kernels: 75.4 us -> 66.5 us  [per_device(): pl.pallas_call(functools.partial(layer_kernel, nz, ny, nt), out_shape=jax...]
where the time goes in v3:
time: 69.6 us; the launch traced here: 69.4 us
  Pallas kernels  66.5 us (96%)
  local copies, waits for them, and re-layouts  1.96 us (3%)
  other arithmetic  0.95 us (1%)
    pallas_call x1, Pallas kernels, per_device(): pl.pallas_call(functools.partial(layer_kernel, nz, ny, nt), out_shape=jax...  66.5 us
    unnamed x1, local copies, waits for them, and re-layouts  1.87 us

profile of v3, /device:TPU:196, one launch (start us, length us, event | category | flops | bytes accessed | tf_op | source)
XLA Modules:
  0.0 69.4 jit_solution(5302414359767569991)
XLA Ops:
  0.0 0.1 add_convert_fusion
  0.1 0.1 mul.60
  0.2 0.2 multiply_cosine_fusion
  0.4 0.6 pad_maximum_fusion.table_ref
  1.1 66.5 %shard_map.73 = bf16[512,512]{1,0:T(8,128)(2,1)} custom-call(s32[8,8]{1,0:T(8,128)} %bitcast.6, s32[8,8]{1,0:T(8,128)} %bitcast.7, f32[2,72,128]{2,1,0:T(8,128)} %pad_maximum_fusion.table_ref, f32[1,1024]{1,0:T(1,128)} %bitcast.8, bf16[512,2048]{1,0:T(8,128)(2,1)} %tokens_hbm.1, bf16[64,2048]{1,0:T(8,128)(2,1)} %bitcast.4, bf16[64,2048]{1,0:T(8,128)(2,1)} %bitcast.5, ...), custom_call_target="tpu_custom_call" | custom-call | tf_op jit(solution)/shard_map/pallas_call | solution.py:441
  67.6 1.9 %copy.9 = bf16[512,512]{1,0:T(8,128)(2,1)} copy(bf16[512,512]{1,0:T(8,128)(2,1)} %shard_map.73) | data formatting | bytes 1048576
  (5 shorter events, 0.0 us)

commit v4 on v3

--- a/solution.py
+++ b/solution.py
@@ -2,6 +2,7 @@
 
 import jax
 import jax.numpy as jnp
+import numpy as np
 from jax import lax
 from jax.experimental import pallas as pl
 from jax.experimental.pallas import tpu as pltpu
@@ -23,7 +24,8 @@
 
 def layer_kernel(
     nz, ny, nt,
-    ids_ref, chosen_ref, table_ref, gain_ref, tokens_hbm, wk_hbm, wv_hbm, wq_hbm, wo_hbm, out_ref,
+    chosen_hbm, gain_hbm, frequency_hbm, tokens_hbm, wk_hbm, wv_hbm, wq_hbm, wo_hbm, out_ref,
+    ids_ref, chosen_ref, gain_ref, frequency_ref, cos_ref, sin_ref,
     tokens, w_pair, w_query, w_out, pairs, query, ga, gb, sa, sb, ra, rb, want, wall, wsm, kv, full,
     load_sem, want_send, want_recv, smem_sem, ring_send, ring_recv,
     a_send, a_recv, b_send, b_recv, tp_send, tp_recv,
@@ -62,14 +64,34 @@
         pl.semaphore_signal(barrier, inc=1, device_id={"tp": peer}, device_id_type=MESH)
 
     loads = [
-        pltpu.make_async_copy(wk_hbm, w_pair.at[pl.ds(0, HD)], load_sem.at[0]),
-        pltpu.make_async_copy(wv_hbm, w_pair.at[pl.ds(HD, HD)], load_sem.at[1]),
-        pltpu.make_async_copy(tokens_hbm, tokens, load_sem.at[2]),
-        pltpu.make_async_copy(wq_hbm, w_query, load_sem.at[3]),
-        pltpu.make_async_copy(wo_hbm, w_out, load_sem.at[4]),
+        pltpu.make_async_copy(source, target, load_sem.at[k])
+        for k, (source, target) in enumerate(
+            (
+                (chosen_hbm, ids_ref),
+                (frequency_hbm, frequency_ref),
+                (wk_hbm, w_pair.at[pl.ds(0, HD)]),
+                (wv_hbm, w_pair.at[pl.ds(HD, HD)]),
+                (tokens_hbm, tokens),
+                (wq_hbm, w_query),
+                (wo_hbm, w_out),
+                (gain_hbm, gain_ref),
+                (chosen_hbm, chosen_ref),
+            )
+        )
     ]
     for load in loads:
         load.start()
+
+    head_lane = lax.broadcasted_iota(jnp.int32, (1, 2 * HD), 1)
+    value_side = head_lane >= HD
+    lower_side = head_lane % HD < HD // 2
+    loads[0].wait()
+    loads[1].wait()
+    place = lax.broadcasted_iota(jnp.int32, (BLK + blocks, 2 * HD), 0)
+    place = jnp.where(place < BLK, place, (me * blocks + place - BLK) * BLK)
+    angles = place.astype(jnp.float32) * frequency_ref[...]
+    cos_ref[...] = jnp.cos(angles)
+    sin_ref[...] = jnp.sin(angles) * jnp.where(lower_side, -1.0, 1.0)
 
     lane = lax.broadcasted_iota(jnp.int32, (blocks, 128), 1)
     found = jnp.full((blocks, 128), -1, jnp.int32)
@@ -79,13 +101,9 @@
         found = jnp.maximum(found, jnp.where(hit, ids % blocks, -1))
     want[...] = jnp.max(found, axis=0, keepdims=True)
 
-    head_lane = lax.broadcasted_iota(jnp.int32, (1, 2 * HD), 1)
-    value_side = head_lane >= HD
-    lower_side = head_lane % HD < HD // 2
-
     def turned(wide, b, only_keys):
-        cos_row, sin_row = table_ref[0, pl.ds(0, BLK)], table_ref[1, pl.ds(0, BLK)]
-        cos_base, sin_base = table_ref[0, pl.ds(BLK + b, 1)], table_ref[1, pl.ds(BLK + b, 1)]
+        cos_row, sin_row = cos_ref[pl.ds(0, BLK)], sin_ref[pl.ds(0, BLK)]
+        cos_base, sin_base = cos_ref[pl.ds(BLK + b, 1)], sin_ref[pl.ds(BLK + b, 1)]
         cosine = cos_base * cos_row - sin_base * sin_row
         sine_wave = sin_base * cos_row + cos_base * sin_row
         if only_keys:
@@ -94,7 +112,7 @@
         other = jnp.where(lower_side, pltpu.roll(wide, 3 * HD // 2, 1), pltpu.roll(wide, HD // 2, 1))
         return wide * cosine + other * sine_wave
 
-    for load in loads[:3]:
+    for load in loads[2:5]:
         load.wait()
     pair = lax.dot_general(
         tokens[...], w_pair[...], (((1,), (1,)), ((), ())), preferred_element_type=jnp.float32
@@ -255,7 +273,7 @@
         for g in now_b:
             start_b(g)
 
-    loads[3].wait()
+    loads[5].wait()
     product = jnp.dot(tokens[...], w_query[...], preferred_element_type=jnp.float32)
     for b in range(blocks):
         for h in range(0, heads, 2):
@@ -266,7 +284,8 @@
             query[h + 1, spot] = jnp.where(
                 value_side, 0.0, pltpu.roll(wide, HD, 1)
             ).astype(jnp.bfloat16)
-    loads[4].wait()
+    for load in loads[6:]:
+        load.wait()
 
     @pl.loop(0, rows)
     def _(p):
@@ -415,22 +434,13 @@
 
 def per_device(tokens, w_query, w_key, w_value, w_out, out_gain, chosen):
     nz, ny, nt = lax.axis_size("kv_0"), lax.axis_size("kv_1"), lax.axis_size("tp")
-    kv_place = lax.axis_index(KV)
     row_count, depth = tokens.shape
     blocks = row_count // BLK
     heads = w_query.shape[1] // HD
     rows, cols = ny * CORES, nz * CORES
     half_size = HD // 2
-    frequency = rope_base ** (-jnp.arange(half_size, dtype=jnp.float32) / half_size)
-    places = jnp.concatenate(
-        [
-            jnp.arange(BLK, dtype=jnp.int32),
-            kv_place * row_count + BLK * jnp.arange(blocks, dtype=jnp.int32),
-        ]
-    )
-    angles = places.astype(jnp.float32)[:, None] * jnp.tile(frequency, 4)[None, :]
-    sign = jnp.where(jnp.arange(2 * HD) % HD < half_size, -1.0, 1.0)
-    table = jnp.stack([jnp.cos(angles), jnp.sin(angles) * sign])
+    frequency = np.float64(rope_base) ** (-np.arange(half_size) / half_size)
+    frequency = jnp.asarray(np.tile(frequency, 4)[None, :], jnp.float32)
 
     piece = (HALF, 2 * HD)
     vmem = pl.BlockSpec(memory_space=pltpu.VMEM)
@@ -441,9 +451,15 @@
     return pl.pallas_call(
         functools.partial(layer_kernel, nz, ny, nt),
         out_shape=jax.ShapeDtypeStruct((row_count, w_out.shape[1]), bf16),
-        in_specs=[vmem, pl.BlockSpec(memory_space=pltpu.SMEM), vmem, vmem] + [far] * 5,
+        in_specs=[far] * 8,
         out_specs=vmem,
         scratch_shapes=[
+            pltpu.VMEM(chosen.shape[1:], jnp.int32),
+            pltpu.SMEM(chosen.shape[1:], jnp.int32),
+            pltpu.VMEM((1, out_gain.shape[0]), jnp.float32),
+            pltpu.VMEM((1, 2 * HD), jnp.float32),
+            pltpu.VMEM((BLK + blocks, 2 * HD), jnp.float32),
+            pltpu.VMEM((BLK + blocks, 2 * HD), jnp.float32),
             pltpu.VMEM((row_count, depth), bf16),
             pltpu.VMEM((2 * HD, depth), bf16),
             pltpu.VMEM(w_query.shape, bf16),
@@ -461,7 +477,7 @@
             pltpu.SMEM((rows + cols, 1, 128), jnp.int32),
             pltpu.VMEM((blocks, SEL * BLK, 2 * HD), bf16),
             pltpu.VMEM((nt, row_count, heads * HD), bf16),
-            dma((5,)),
+            dma((9,)),
             dma, dma, dma,
             dma((2, 2, steps)),
             dma((2, 2, steps)),
@@ -472,10 +488,15 @@
             dma((3, blocks)),
             dma((3, blocks)),
         ],
-        compiler_params=pltpu.CompilerParams(collective_id=0, has_side_effects=True),
+        compiler_params=pltpu.CompilerParams(collective_id=0, has_side_effects=True, vmem_limit_bytes=40*2**20),
     )(
-        chosen[0], chosen[0], table, out_gain[None, :],
-        tokens, w_key.T, w_value.T, w_query, w_out,
+        *(
+            pltpu.with_memory_space_constraint(a, pltpu.HBM)
+            for a in (
+                chosen[0], out_gain[None, :], frequency,
+                tokens, w_key.T, w_value.T, w_query, w_out,
+            )
+        )
     )
 
 

time: 69.6 us -> 65.8 us (0.945)
  Pallas kernels: 66.5 us -> 64.9 us
  local copies, waits for them, and re-layouts: 1.96 us -> 0.8 us
  other arithmetic: 0.95 us -> 0 us
    pallas_call x1, Pallas kernels: 66.5 us -> 64.9 us  [per_device(): pl.pallas_call(functools.partial(layer_kernel, nz, ny, nt), out_shape=jax...]
    unnamed x1, local copies, waits for them, and re-layouts: 1.87 us -> 0.8 us
where the time goes in v4:
time: 65.8 us; the launch traced here: 65.7 us
  Pallas kernels  64.9 us (99%)
  local copies, waits for them, and re-layouts  0.8 us (1%)
    pallas_call x1, Pallas kernels, per_device(): pl.pallas_call(functools.partial(layer_kernel, nz, ny, nt), out_shape=jax...  64.9 us

profile of v4, /device:TPU:196, one launch (start us, length us, event | category | flops | bytes accessed | tf_op | source)
XLA Modules:
  0.0 65.7 jit_solution(9401043482331096559)
XLA Ops:
  0.0 64.9 %shard_map.82 = bf16[512,512]{1,0:T(8,128)(2,1)S(1)} custom-call(s32[8,8]{1,0:T(8,128)} %bitcast.6, f32[1,1024]{1,0:T(1,128)} %bitcast.7, f32[1,128]{1,0:T(1,128)} %constant.2.clone.frequency_hbm, bf16[512,2048]{1,0:T(8,128)(2,1)} %tokens_hbm.1, bf16[64,2048]{1,0:T(8,128)(2,1)} %bitcast.4, bf16[64,2048]{1,0:T(8,128)(2,1)} %bitcast.5, ...), custom_call_target="tpu_custom_call" | custom-call | tf_op jit(solution)/shard_map/pallas_call | solution.py:451
  64.9 0.8 %copy.10 = bf16[512,512]{1,0:T(8,128)(2,1)} copy(bf16[512,512]{1,0:T(8,128)(2,1)S(1)} %shard_map.82) | data formatting | bytes 1048576

commit v5 on v4

--- a/solution.py
+++ b/solution.py
@@ -304,7 +304,6 @@
                 part = pl.ds(lo, hi - lo)
                 pltpu.make_async_copy(sb.at[p, part], rb.at[p, part], b_recv.at[g, p]).wait()
 
-    lag = 3
     out_rows = 2 * BLK
     key_lane = lax.broadcasted_iota(jnp.int32, (1, SEL * BLK), 1)
     query_row = lax.broadcasted_iota(jnp.int32, (BLK, SEL * BLK), 0)
@@ -379,9 +378,7 @@
         full[t, pl.ds(b * BLK, BLK)] = attend_block(b)
         near(0, b).start()
         near(1, b).start()
-        if b >= lag:
-            pass_on(b - lag)
-    for b in range(blocks - lag, blocks):
+    for b in range(blocks):
         pass_on(b)
 
     width = heads * HD

time: 65.8 us -> 64.3 us (0.977)
  the two profiles are of different devices: /device:TPU:196 before, /device:TPU:192 now
where the time goes in v5:
time: 64.3 us; the launch traced here: 64.2 us
  Pallas kernels  63.4 us (99%)
  local copies, waits for them, and re-layouts  0.8 us (1%)
    pallas_call x1, Pallas kernels, per_device(): pl.pallas_call(functools.partial(layer_kernel, nz, ny, nt), out_shape=jax...  63.4 us

profile of v5, /device:TPU:192, one launch (start us, length us, event | category | flops | bytes accessed | tf_op | source)
XLA Modules:
  0.0 64.2 jit_solution(11287315429087999252)
XLA Ops:
  0.0 63.4 %shard_map.82 = bf16[512,512]{1,0:T(8,128)(2,1)S(1)} custom-call(s32[8,8]{1,0:T(8,128)} %bitcast.6, f32[1,1024]{1,0:T(1,128)} %bitcast.7, f32[1,128]{1,0:T(1,128)} %constant.2.clone.frequency_hbm, bf16[512,2048]{1,0:T(8,128)(2,1)} %tokens_hbm.1, bf16[64,2048]{1,0:T(8,128)(2,1)} %bitcast.4, bf16[64,2048]{1,0:T(8,128)(2,1)} %bitcast.5, ...), custom_call_target="tpu_custom_call" | custom-call | tf_op jit(solution)/shard_map/pallas_call | solution.py:448
  63.4 0.8 %copy.10 = bf16[512,512]{1,0:T(8,128)(2,1)} copy(bf16[512,512]{1,0:T(8,128)(2,1)S(1)} %shard_map.82) | data formatting | bytes 1048576

commit v6 on v5

--- a/solution.py
+++ b/solution.py
@@ -217,9 +217,14 @@
 
         @pl.when(needed_a(g))
         def _():
-            @pl.loop(1, rows)
-            def _(d):
-                send_a(d, g).start()
+            if g == 0:
+                @pl.loop(1, rows - row_me)
+                def _(d):
+                    send_a(d, g).start()
+            else:
+                @pl.loop(1, rows)
+                def _(d):
+                    send_a(d, g).start()
 
             pltpu.make_async_copy(
                 sa.at[row_me, part], ra.at[row_me, part], a_recv.at[g, row_me]
@@ -245,7 +250,7 @@
     last = max(nz, ny) // 2
 
     def ring_step(step):
-        for axis, size in ((0, nz), (1, ny)):
+        for axis, size in ((1, ny), (0, nz)):
             for way, count in ((0, size // 2), (1, (size - 1) // 2)):
                 if 0 < step <= count:
                     hops[axis, way, step - 1].wait_recv()
@@ -292,7 +297,7 @@
         for g, (lo, hi) in enumerate(groups_a):
             part = pl.ds(lo, hi - lo)
 
-            @pl.when(needed_a(g))
+            @pl.when(p <= row_me if g == 0 else needed_a(g))
             def _():
                 pltpu.make_async_copy(sa.at[p, part], ra.at[p, part], a_recv.at[g, p]).wait()
 
@@ -410,7 +415,7 @@
     @pl.loop(1, rows)
     def _(d):
         for g in range(len(groups_a)):
-            @pl.when(needed_a(g))
+            @pl.when(d < rows - row_me if g == 0 else needed_a(g))
             def _():
                 send_a(d, g).wait_send()
 

time: 64.3 us -> 62.3 us (0.969)
  the two profiles are of different devices: /device:TPU:192 before, /device:TPU:208 now
where the time goes in v6:
time: 62.3 us; the launch traced here: 62.2 us
  Pallas kernels  61.4 us (99%)
  local copies, waits for them, and re-layouts  0.8 us (1%)
    pallas_call x1, Pallas kernels, per_device(): pl.pallas_call(functools.partial(layer_kernel, nz, ny, nt), out_shape=jax...  61.4 us

profile of v6, /device:TPU:208, one launch (start us, length us, event | category | flops | bytes accessed | tf_op | source)
XLA Modules:
  0.0 62.2 jit_solution(9625272261948022845)
XLA Ops:
  0.0 61.4 %shard_map.82 = bf16[512,512]{1,0:T(8,128)(2,1)S(1)} custom-call(s32[8,8]{1,0:T(8,128)} %bitcast.6, f32[1,1024]{1,0:T(1,128)} %bitcast.7, f32[1,128]{1,0:T(1,128)} %constant.2.clone.frequency_hbm, bf16[512,2048]{1,0:T(8,128)(2,1)} %tokens_hbm.1, bf16[64,2048]{1,0:T(8,128)(2,1)} %bitcast.4, bf16[64,2048]{1,0:T(8,128)(2,1)} %bitcast.5, ...), custom_call_target="tpu_custom_call" | custom-call | tf_op jit(solution)/shard_map/pallas_call | solution.py:453
  61.4 0.8 %copy.10 = bf16[512,512]{1,0:T(8,128)(2,1)} copy(bf16[512,512]{1,0:T(8,128)(2,1)S(1)} %shard_map.82) | data formatting | bytes 1048576

commit v7 on v6

--- a/solution.py
+++ b/solution.py
@@ -309,7 +309,7 @@
                 part = pl.ds(lo, hi - lo)
                 pltpu.make_async_copy(sb.at[p, part], rb.at[p, part], b_recv.at[g, p]).wait()
 
-    out_rows = 2 * BLK
+    out_rows = BLK
     key_lane = lax.broadcasted_iota(jnp.int32, (1, SEL * BLK), 1)
     query_row = lax.broadcasted_iota(jnp.int32, (BLK, SEL * BLK), 0)
     key_col = lax.broadcasted_iota(jnp.int32, (BLK, SEL * BLK), 1)

time: 62.3 us -> 62.9 us (level)
  no operation moved by 1% of the time
where the time goes in v7:
time: 62.9 us; the launch traced here: 62.8 us
  Pallas kernels  62 us (99%)
  local copies, waits for them, and re-layouts  0.8 us (1%)
    pallas_call x1, Pallas kernels, per_device(): pl.pallas_call(functools.partial(layer_kernel, nz, ny, nt), out_shape=jax...  62 us

profile of v7, /device:TPU:208, one launch (start us, length us, event | category | flops | bytes accessed | tf_op | source)
XLA Modules:
  0.0 62.8 jit_solution(13134703888417265726)
XLA Ops:
  0.0 62.0 %shard_map.82 = bf16[512,512]{1,0:T(8,128)(2,1)S(1)} custom-call(s32[8,8]{1,0:T(8,128)} %bitcast.6, f32[1,1024]{1,0:T(1,128)} %bitcast.7, f32[1,128]{1,0:T(1,128)} %constant.2.clone.frequency_hbm, bf16[512,2048]{1,0:T(8,128)(2,1)} %tokens_hbm.1, bf16[64,2048]{1,0:T(8,128)(2,1)} %bitcast.4, bf16[64,2048]{1,0:T(8,128)(2,1)} %bitcast.5, ...), custom_call_target="tpu_custom_call" | custom-call | tf_op jit(solution)/shard_map/pallas_call | solution.py:453
  62.0 0.8 %copy.10 = bf16[512,512]{1,0:T(8,128)(2,1)} copy(bf16[512,512]{1,0:T(8,128)(2,1)S(1)} %shard_map.82) | data formatting | bytes 1048576
